TPU v7x, 32 devices: a whole 2x2x4 slice. The times are simulated.
32 devices in a mesh: grp: 2 (over x), sp: 4 (over y, core), tp: 4 (over z).
Axes of the slice: x: 2, y: 2, z: 4, core: 2. Of those that a mesh axis runs over, the one named last changes fastest.
Arguments:
- tokens: bfloat16 [8, 1024, 2048], P(('grp', 'tp'), 'sp'), parts along dimension 0, may hold values from -6 to 6
- kv_down: bfloat16 [2048, 512], replicated, may hold values from -0.125 to 0.125
- rope_down: bfloat16 [2048, 64], replicated, may hold values from -0.125 to 0.125
- kv_gain: float32 [512], replicated, may hold values from 0.1 to 1.9
- key_up: bfloat16 [512, 16, 128], replicated, may hold values from -0.25 to 0.25
- value_up: bfloat16 [512, 16, 128], replicated, may hold values from -0.25 to 0.25
- query_nope: bfloat16 [8, 16, 128], P(('grp', 'sp'), 'tp'), parts along dimension 0, may hold values from -180 to 180
- query_rope: bfloat16 [8, 16, 64], P(('grp', 'sp'), 'tp'), parts along dimension 0, may hold values from -180 to 180
Outputs:
- key_cache: bfloat16 [8, 16, 1024, 128], P(('grp', 'sp'), 'tp'), parts along dimension 0
- value_cache: bfloat16 [8, 16, 1024, 128], P(('grp', 'sp'), 'tp'), parts along dimension 0
- rope_cache: bfloat16 [8, 1024, 64], P(('grp', 'sp')), parts along dimension 0
- read_out: bfloat16 [8, 16, 128], P(('grp', 'sp'), 'tp'), parts along dimension 0
There are 2 independent parts, one for each index of `grp`. A program takes and returns all parts, laid end to end along the dimension named above; an argument that names none is the same for every part. Nothing has to cross between parts.
All inputs are finite; a program needn't handle non-finite values.
Results may differ from a plain program's by a relative error of at most 0.018.
The roundings to bfloat16 on the way count: a program that leaves them out, or rounds other values in their place, can miss the bound.
Values may be sent and summed in bfloat16 or wider, within the bound.
A program may use at most 64 MiB of HBM per device.

v0:
```python
import functools

import jax
import jax.numpy as jnp
import numpy as np
from jax import lax
from jax.experimental import pallas as pl
from jax.experimental.pallas import tpu as pltpu
from jax.sharding import PartitionSpec as P

norm_epsilon = 1e-06
rope_base = 10000.0
MESH = pl.DeviceIdType.MESH
F32, BF16 = jnp.float32, jnp.bfloat16


def tables(length, width):
    frequency = (1.0 / rope_base ** (np.arange(0, width, 2, dtype=np.float64) / width)).astype(np.float32)
    angles = frequency[:, None] * np.arange(length, dtype=np.float32)[None, :]
    cached = np.stack([np.cos(angles.astype(np.float64)), np.sin(angles.astype(np.float64))])
    ask = (np.float32(length) * frequency).astype(np.float64)
    asked = np.stack([np.tile(np.cos(ask), 2), np.tile(np.sin(ask), 2)])
    return cached.astype(np.float32), asked.astype(np.float32)


def kernel(
    sp_count, tp_count, heads_dev, bounds,
    tok, kvd, rpt, gain, kup, vup, tab,
    key_out, val_out, rope_out,
    box, tok_v, kvd_v, rpt_v, gain_v, up_v, wide, kw, vw, tab_v,
    in_sem, zsend, zrecv, csend, crecv,
):
    me = lax.axis_index("sp")
    here = lax.axis_index("tp")
    seq_local, pos_dev, _ = tok.shape
    rope_width = rpt.shape[0]
    half = rope_width // 2
    key_width = kup.shape[2]
    rope_rows = bounds[0]
    pieces = [pl.ds(a, b - a) for a, b in zip((0,) + bounds[1:-1], bounds[1:])]
    count = len(pieces)
    last = tp_count - 1

    barrier = pltpu.get_barrier_semaphore()
    for step in range(1, sp_count):
        pl.semaphore_signal(
            barrier, inc=1, device_id={"sp": lax.rem(me + step, sp_count)}, device_id_type=MESH
        )
    if tp_count > 1:
        for step in (1, last):
            pl.semaphore_signal(
                barrier, inc=1, device_id={"tp": lax.rem(here + step, tp_count)}, device_id_type=MESH
            )

    tile = up_v.shape[2]
    head_start = here * heads_dev
    head_tile = pl.multiple_of(head_start // tile * tile, tile)
    head_off = lax.rem(head_start, tile)
    loads = [
        pltpu.make_async_copy(src, dst, in_sem.at[n])
        for n, (src, dst) in enumerate([
            (tok, tok_v),
            (kvd, kvd_v),
            (gain, gain_v),
            (rpt, rpt_v),
            (tab.at[:, :, pl.ds(pl.multiple_of(me * pos_dev, pos_dev), pos_dev)], tab_v),
            (kup.at[:, pl.ds(head_tile, tile), :], up_v.at[0]),
            (vup.at[:, pl.ds(head_tile, tile), :], up_v.at[1]),
        ])
    ]
    for load in loads:
        load.start()

    def slot(prompt):
        return jnp.where(prompt == me, me, sp_count + prompt)

    for n in (3, 4, 0):
        loads[n].wait()
    for q in range(seq_local):
        mine = slot(here * seq_local + q)
        rows = tok_v[q]
        raw = lax.dot_general(rpt_v[...], rows, (((1,), (1,)), ((), ())), preferred_element_type=F32)
        cosine, sine_part = tab_v[0], tab_v[1]
        front, back = raw[:half], raw[half:]
        turned = jnp.concatenate(
            [front * cosine - back * sine_part, front * sine_part + back * cosine], axis=0
        ).astype(BF16)
        groups = rope_width // rope_rows
        box[mine, 0:rope_rows, :] = jnp.concatenate(
            [turned[g * rope_rows:(g + 1) * rope_rows] for g in range(groups)], axis=1
        )
    def along(prompt, way, hop, q, s):
        part = box.at[slot(prompt), pieces[s]]
        return pltpu.make_async_remote_copy(
            src_ref=part, dst_ref=part,
            send_sem=zsend.at[way, hop, q, s], recv_sem=zrecv.at[way, hop, q, s],
            device_id={"tp": here + (1 if way == 0 else -1)}, device_id_type=MESH,
        )

    def across(prompt, s):
        return pltpu.make_async_remote_copy(
            src_ref=box.at[slot(prompt), pieces[s]], dst_ref=box.at[me, pieces[s]],
            send_sem=csend.at[prompt, s], recv_sem=crecv.at[me, s],
            device_id={"sp": prompt}, device_id_type=MESH,
        )

    inner = {0: here < last, 1: here > 0}
    for n in (1, 2):
        loads[n].wait()
    half_rows = pos_dev // 2
    for group in range(2):
        for q in range(seq_local):
            mine = slot(here * seq_local + q)
            latent = jnp.dot(
                tok_v[q, group * half_rows:(group + 1) * half_rows, :], kvd_v[...],
                preferred_element_type=F32,
            )
            normed = (
                latent
                * lax.rsqrt(jnp.mean(latent * latent, axis=-1, keepdims=True) + norm_epsilon)
                * gain_v[...]
            ).astype(BF16)
            begin = rope_rows + group * half_rows
            box[mine, begin:begin + half_rows, :] = normed
        if group == 0:
            pl.semaphore_wait(barrier, sp_count - 1 + (2 if tp_count > 1 else 0))
        for q in range(seq_local):
            prompt = here * seq_local + q
            for s in ((0,) if group == 0 else range(1, count)):
                for way in (0, 1):
                    @pl.when(inner[way])
                    def _(way=way, s=s):
                        along(prompt, way, 0, q, s).start()

                @pl.when(prompt != me)
                def _(s=s):
                    across(prompt, s).start()

    for n in (5, 6):
        loads[n].wait()
    depth = up_v.shape[1]
    for n, target in enumerate((kw, vw)):
        wide[...] = up_v[n].astype(F32).reshape(depth * tile, key_width)
        for h in range(heads_dev):
            target[:, h * key_width:(h + 1) * key_width] = wide[
                pl.ds(head_off + h, depth, stride=tile), :
            ].astype(BF16)

    for hop in range(last):
        for q in range(seq_local):
            for s in range(count):
                for way in (0, 1):
                    owner = here - 1 - hop if way == 0 else here + 1 + hop
                    has = owner >= 0 if way == 0 else owner <= last

                    @pl.when(has)
                    def _(way=way, s=s, owner=owner):
                        prompt = owner * seq_local + q
                        along(prompt, way, hop, q, s).wait_recv()
                        if hop + 1 < last:
                            @pl.when(inner[way])
                            def _():
                                along(prompt, way, hop + 1, q, s).start()

                        @pl.when(prompt != me)
                        def _():
                            across(prompt, s).start()

    group_rows = pos_dev // 2
    for group in range(2):
        for step in range(sp_count):
            source = lax.rem(me + step, sp_count)
            if step:
                for s in ((0,) if group == 0 else range(1, count)):
                    part = box.at[source, pieces[s]]
                    pltpu.make_async_remote_copy(
                        src_ref=part, dst_ref=part,
                        send_sem=csend.at[source, s], recv_sem=crecv.at[source, s],
                        device_id={"sp": source}, device_id_type=MESH,
                    ).wait_recv()
            block = pl.ds(pl.multiple_of(source * pos_dev, pos_dev), pos_dev)
            if group == 0:
                packed = box[source, 0:rope_rows, :]
                turned = jnp.concatenate(
                    [packed[:, g * pos_dev:(g + 1) * pos_dev] for g in range(rope_width // rope_rows)], axis=0
                )
                rope_out[0, :, block] = turned
            begin = rope_rows + group * group_rows
            rows = box[source, begin:begin + group_rows, :]
            place = pl.ds(pl.multiple_of(source * pos_dev + group * group_rows, group_rows), group_rows)
            keys = jnp.dot(rows, kw[...], preferred_element_type=F32).astype(BF16)
            values = jnp.dot(rows, vw[...], preferred_element_type=F32).astype(BF16)
            for h in range(heads_dev):
                key_out[0, h, place, :] = keys[:, h * key_width:(h + 1) * key_width]
                val_out[0, h, place, :] = values[:, h * key_width:(h + 1) * key_width]

    for hop in range(last):
        for q in range(seq_local):
            for s in range(count):
                for way in (0, 1):
                    owner = here - hop if way == 0 else here + hop
                    has = owner >= 0 if way == 0 else owner <= last

                    @pl.when(jnp.logical_and(has, inner[way]))
                    def _(way=way, s=s, owner=owner):
                        along(owner * seq_local + q, way, hop, q, s).wait_send()
    for step in range(1, sp_count):
        prompt = lax.rem(me + step, sp_count)
        for s in range(count):
            across(prompt, s).wait_send()


def finish(scale, keys, vals, ropes, query, ask, qtab, key_out, val_out, rope_out, read_out, sem):
    moves = [
        pltpu.make_async_copy(src, dst, sem.at[n])
        for n, (src, dst) in enumerate([(vals, val_out), (keys, key_out), (ropes, rope_out)])
    ]
    for move in moves:
        move.start()
    heads_dev = query.shape[1]
    half = ask.shape[2] // 2
    turn = ask[0].astype(F32)
    swapped = jnp.concatenate([-turn[:, half:], turn[:, :half]], axis=1)
    rotated = (turn * qtab[0:1, :] + swapped * qtab[1:2, :]).astype(BF16)
    asked = query[0]
    picks = []
    for h in range(heads_dev):
        full = lax.dot_general(
            asked, keys[0, h], (((1,), (1,)), ((), ())), preferred_element_type=F32
        )
        picks.append(full[h:h + 1])
    total = jnp.concatenate(picks, axis=0)
    total = (total + jnp.dot(rotated, ropes[0], preferred_element_type=F32)) * scale
    terms = jnp.exp(total - jnp.max(total, axis=-1, keepdims=True))
    weights = terms / jnp.sum(terms, axis=-1, keepdims=True)
    high = weights.astype(BF16).astype(F32)
    both = jnp.concatenate([high, weights - high], axis=0).astype(BF16)
    reads = []
    for h in range(heads_dev):
        read = jnp.dot(both, vals[0, h], preferred_element_type=F32)
        reads.append(read[h:h + 1] + read[heads_dev + h:heads_dev + h + 1])
    read_out[0] = jnp.concatenate(reads, axis=0).astype(BF16)
    for move in moves:
        move.wait()


def local(tokens, kv_down, rope_down, kv_gain, key_up, value_up, query_nope, query_rope):
    seq_local, pos_dev, model_width = tokens.shape
    sp_count = lax.axis_size("sp")
    tp_count = lax.axis_size("tp")
    latent_width = kv_down.shape[1]
    rope_width = rope_down.shape[1]
    head_count, key_width = key_up.shape[1], key_up.shape[2]
    heads_dev = head_count // tp_count
    length = pos_dev * sp_count
    rope_rows = rope_width * pos_dev // latent_width
    rows = rope_rows + pos_dev
    bounds = (rope_rows, rope_rows + pos_dev // 2, rope_rows + pos_dev * 3 // 4, rows)
    prompts = tp_count * seq_local
    cached, asked = tables(length, rope_width)
    tile = 8
    any_space = pl.BlockSpec(memory_space=pl.ANY)
    vmem = pl.BlockSpec(memory_space=pltpu.VMEM)
    hops = max(tp_count - 1, 1)
    count = len(bounds) - 1
    dma = pltpu.SemaphoreType.DMA
    parts = pl.pallas_call(
        functools.partial(kernel, sp_count, tp_count, heads_dev, bounds),
        out_shape=(
            jax.ShapeDtypeStruct((1, heads_dev, length, key_width), BF16),
            jax.ShapeDtypeStruct((1, heads_dev, length, key_width), BF16),
            jax.ShapeDtypeStruct((1, rope_width, length), BF16),
        ),
        in_specs=[any_space] * 7,
        out_specs=(vmem,) * 3,
        scratch_shapes=[
            pltpu.VMEM((sp_count + prompts, rows, latent_width), BF16),
            pltpu.VMEM(tokens.shape, BF16),
            pltpu.VMEM(kv_down.shape, BF16),
            pltpu.VMEM((rope_width, model_width), BF16),
            pltpu.VMEM((1, latent_width), F32),
            pltpu.VMEM((2, latent_width, tile, key_width), BF16),
            pltpu.VMEM((latent_width * tile, key_width), F32),
            pltpu.VMEM((latent_width, heads_dev * key_width), BF16),
            pltpu.VMEM((latent_width, heads_dev * key_width), BF16),
            pltpu.VMEM((2, rope_width // 2, pos_dev), F32),
            dma((7,)),
            dma((2, hops, seq_local, count)),
            dma((2, hops, seq_local, count)),
            dma((prompts, count)),
            dma((sp_count, count)),
        ],
        compiler_params=pltpu.CompilerParams(
            collective_id=0, has_side_effects=True, vmem_limit_bytes=53000000
        ),
    )(
        tokens, kv_down, rope_down.T, kv_gain.reshape(1, latent_width), key_up, value_up,
        jnp.asarray(cached),
    )
    key_cache, value_cache, rope_t, read_out = pl.pallas_call(
        functools.partial(finish, (key_width + rope_width) ** (-0.5)),
        out_shape=tuple(jax.ShapeDtypeStruct(part.shape, BF16) for part in parts)
        + (jax.ShapeDtypeStruct((1, heads_dev, key_width), BF16),),
        in_specs=[vmem] * 6,
        out_specs=(any_space,) * 3 + (vmem,),
        scratch_shapes=[dma((3,))],
        compiler_params=pltpu.CompilerParams(vmem_limit_bytes=8 * 1024 * 1024),
    )(*parts, query_nope, query_rope, jnp.asarray(asked))
    return (key_cache, value_cache, jnp.swapaxes(rope_t, 1, 2), read_out)


def solution(mesh):
    placed = (
        P(("grp", "tp"), "sp", None),
        P(),
        P(),
        P(),
        P(),
        P(),
        P(("grp", "sp"), "tp", None),
        P(("grp", "sp"), "tp", None),
    )
    return jax.shard_map(
        local,
        mesh=mesh,
        in_specs=placed,
        out_specs=(
            P(("grp", "sp"), "tp", None, None),
            P(("grp", "sp"), "tp", None, None),
            P(("grp", "sp"), None, None),
            P(("grp", "sp"), "tp", None),
        ),
        check_vma=False,
    )
```

profile of v0, /device:TPU:5, one launch (start us, length us, event | category | flops | bytes accessed | tf_op | source)
XLA Modules:
  0.0 35.1 jit_solution(16712335995729884157)
XLA Ops:
  0.6 0.0 copy-start
  0.6 0.9 %copy-done = bf16[2048,64]{0,1:T(8,128)(2,1)S(1)} copy-done((bf16[2048,64]{0,1:T(8,128)(2,1)S(1)}, bf16[2048,64]{0,1:T(8,128)(2,1)}, u32[]{:S(2)}) %copy-start) | copy-done | bytes 262168
  1.6 0.0 copy-start.1
  1.6 0.9 %copy-done.1 = f32[2,32,1024]{2,1,0:T(8,128)S(1)} copy-done((f32[2,32,1024]{2,1,0:T(8,128)S(1)}, f32[2,32,1024]{2,1,0:T(8,128)}, u32[]{:S(2)}) %copy-start.1) | copy-done | bytes 262168
  2.5 0.0 copy-start.2
  2.5 0.7 %copy-done.2 = f32[512]{0:T(512)S(1)} copy-done((f32[512]{0:T(512)S(1)}, f32[512]{0:T(512)}, u32[]{:S(2)}) %copy-start.2) | copy-done | bytes 2072
  3.2 0.0 copy-start.3
  3.2 0.0 copy-start.4
  3.2 0.0 copy-start.5
  3.2 29.7 %shard_map.129 = (bf16[1,4,1024,128]{3,2,1,0:T(8,128)(2,1)S(1)}, bf16[1,4,1024,128]{3,2,1,0:T(8,128)(2,1)S(1)}, bf16[1,64,1024]{2,1,0:T(8,128)(2,1)S(1)}) custom-call(bf16[1,256,2048]{2,1,0:T(8,128)(2,1)} %tok.1, bf16[2048,512]{1,0:T(8,128)(2,1)} %kvd.1, bf16[64,2048]{1,0:T(8,128)(2,1)S(1)} %bitcast.3, f32[1,512]{1,0:T(1,128)S(1)} %bitcast.4, ...), custom_call_target="tpu_custom_call" | custom-call | tf_op jit(solution)/shard_map/pallas_call | solution.py:267
  32.9 0.0 copy-done.3
  32.9 0.0 copy-done.4
  32.9 0.0 copy-done.5
  32.9 2.2 %shard_map.130 = (bf16[1,4,1024,128]{3,2,1,0:T(8,128)(2,1)}, bf16[1,4,1024,128]{3,2,1,0:T(8,128)(2,1)}, bf16[1,64,1024]{2,1,0:T(8,128)(2,1)}, bf16[1,4,128]{2,1,0:T(4,128)(2,1)}) custom-call(bf16[1,4,1024,128]{3,2,1,0:T(8,128)(2,1)S(1)} %get-tuple-element.11.keys, bf16[1,4,1024,128]{3,2,1,0:T(8,128)(2,1)S(1)} %get-tuple-element.12.vals, ...), custom_call_target="tpu_custom_call" | custom-call | tf_op jit(solution)/shard_map/pallas_call | solution.py:300
Async XLA Ops:
  0.6 1.0 %copy-start = (bf16[2048,64]{0,1:T(8,128)(2,1)S(1)}, bf16[2048,64]{0,1:T(8,128)(2,1)}, u32[]{:S(2)}) copy-start(bf16[2048,64]{0,1:T(8,128)(2,1)} %param.12) | copy-start | bytes 786436
  1.6 0.9 %copy-start.1 = (f32[2,32,1024]{2,1,0:T(8,128)S(1)}, f32[2,32,1024]{2,1,0:T(8,128)}, u32[]{:S(2)}) copy-start(f32[2,32,1024]{2,1,0:T(8,128)} %constant.4.clone.tab) | copy-start | bytes 786436
  2.5 0.7 %copy-start.2 = (f32[512]{0:T(512)S(1)}, f32[512]{0:T(512)}, u32[]{:S(2)}) copy-start(f32[512]{0:T(512)} %param.13) | copy-start | bytes 6148
  3.2 29.7 %copy-start.3 = (bf16[1,4,128]{2,1,0:T(4,128)(2,1)S(1)}, bf16[1,4,128]{2,1,0:T(4,128)(2,1)}, u32[]{:S(2)}) copy-start(bf16[1,4,128]{2,1,0:T(4,128)(2,1)} %query.1) | copy-start | bytes 3076
  3.2 29.7 %copy-start.4 = (bf16[1,4,64]{2,1,0:T(4,128)(2,1)S(1)}, bf16[1,4,64]{2,1,0:T(4,128)(2,1)}, u32[]{:S(2)}) copy-start(bf16[1,4,64]{2,1,0:T(4,128)(2,1)} %ask.1) | copy-start | bytes 1540
  3.2 29.7 %copy-start.5 = (f32[2,64]{1,0:T(2,128)S(1)}, f32[2,64]{1,0:T(2,128)}, u32[]{:S(2)}) copy-start(f32[2,64]{1,0:T(2,128)} %constant.5.clone.qtab) | copy-start | bytes 1540
where the time goes:
time: 35.3 us; the launch traced here: 35.1 us
  Pallas kernels  31.9 us (90%)
  local copies, waits for them, and re-layouts  2.58 us (7%)
  between operations  0.68 us (2%)
    pallas_call x1, Pallas kernels, local(): pl.pallas_call(functools.partial(kernel, sp_count, tp_count, heads_dev, b...  29.7 us
    unnamed x12, local copies, waits for them, and re-layouts  2.58 us
    pallas_call x1, Pallas kernels, local(): pl.pallas_call(functools.partial(finish, (key_width + rope_width) ** (-0....  2.17 us

commit v1 on v0

v1 whole, which is shorter than its diff:
```python
import functools

import jax
import jax.numpy as jnp
import numpy as np
from jax import lax
from jax.experimental import pallas as pl
from jax.experimental.pallas import tpu as pltpu
from jax.sharding import PartitionSpec as P

norm_epsilon = 1e-06
rope_base = 10000.0
MESH = pl.DeviceIdType.MESH
F32, BF16 = jnp.float32, jnp.bfloat16


def tables(length, width):
    frequency = (1.0 / rope_base ** (np.arange(0, width, 2, dtype=np.float64) / width)).astype(np.float32)
    angles = frequency[:, None] * np.arange(length, dtype=np.float32)[None, :]
    cached = np.stack([np.cos(angles.astype(np.float64)), np.sin(angles.astype(np.float64))])
    ask = (np.float32(length) * frequency).astype(np.float64)
    asked = np.stack([np.tile(np.cos(ask), 2), np.tile(np.sin(ask), 2)])
    return cached.astype(np.float32), asked.astype(np.float32)


def kernel(
    sp_count, tp_count, heads_dev, cuts, parts,
    tok, kvd, rpt, gain, kup, vup, tab,
    key_out, val_out, rope_out,
    box, tok_v, kvd_v, rpt_v, gain_v, up_v, wide, kw, vw, tab_v,
    first_sem, in_sem, zsend, zrecv, csend, crecv,
):
    me = lax.axis_index("sp")
    here = lax.axis_index("tp")
    seq_local, pos_dev, model_width = tok.shape
    rope_width = rpt.shape[0]
    half = rope_width // 2
    key_width = kup.shape[2]
    rope_rows = box.shape[1] - pos_dev
    rope_packs = rope_width // rope_rows
    pieces = [pl.ds(a, b - a) for a, b in zip(cuts[:-1], cuts[1:])]
    count = len(pieces)
    last = tp_count - 1
    inner = {0: here < last, 1: here > 0}
    ends = {0: here == last, 1: here == 0}
    near_end = {0: here + 1 == last, 1: here - 1 == 0}
    at_end = jnp.logical_or(here == 0, here == last)

    half_rows = pos_dev // 2
    starts = (0, half_rows + rope_rows)
    halves = ([s for s in range(count) if cuts[s] < half_rows], [s for s in range(count) if cuts[s] >= half_rows])

    barrier = pltpu.get_barrier_semaphore()
    for step in range(1, sp_count):
        pl.semaphore_signal(
            barrier, inc=1, device_id={"sp": lax.rem(me + step, sp_count)}, device_id_type=MESH
        )
    for way in (0, 1):
        @pl.when(inner[way])
        def _(way=way):
            for step in range(sp_count):
                pl.semaphore_signal(
                    barrier, inc=1,
                    device_id={"sp": lax.rem(me + step, sp_count), "tp": here + (1 if way == 0 else -1)},
                    device_id_type=MESH,
                )

    tile = up_v.shape[2]
    head_start = here * heads_dev
    head_tile = pl.multiple_of(head_start // tile * tile, tile)
    head_off = lax.rem(head_start, tile)
    deep = model_width // parts
    firsts = []
    for n in range(parts):
        span = pl.ds(n * deep, deep)
        firsts.append([
            pltpu.make_async_copy(src, dst, first_sem.at[n, m])
            for m, (src, dst) in enumerate([
                (kvd.at[span, :], kvd_v.at[span, :]),
                (tok.at[:, 0:half_rows, span], tok_v.at[:, 0:half_rows, span]),
            ])
        ])
    for pair in firsts:
        for load in pair:
            load.start()
    loads = [
        pltpu.make_async_copy(src, dst, in_sem.at[n])
        for n, (src, dst) in enumerate([
            (gain, gain_v),
            (tok.at[:, half_rows:pos_dev, :], tok_v.at[:, half_rows:pos_dev, :]),
            (rpt, rpt_v),
            (tab.at[:, :, pl.ds(pl.multiple_of(me * pos_dev, pos_dev), pos_dev)], tab_v),
            (kup.at[:, pl.ds(head_tile, tile), :], up_v.at[0]),
            (vup.at[:, pl.ds(head_tile, tile), :], up_v.at[1]),
        ])
    ]
    for load in loads:
        load.start()

    def slot(prompt):
        return jnp.where(prompt == me, me, sp_count + prompt)

    def along(prompt, way, hop, q, s, final=False):
        part = box.at[slot(prompt), pieces[s]]
        tp = here + (1 if way == 0 else -1)
        if final:
            return pltpu.make_async_remote_copy(
                src_ref=part, dst_ref=box.at[me, pieces[s]],
                send_sem=zsend.at[way, hop, q, s], recv_sem=crecv.at[me, s],
                device_id={"sp": prompt, "tp": tp}, device_id_type=MESH,
            )
        return pltpu.make_async_remote_copy(
            src_ref=part, dst_ref=part,
            send_sem=zsend.at[way, hop, q, s], recv_sem=zrecv.at[way, hop, q, s],
            device_id={"sp": me, "tp": tp}, device_id_type=MESH,
        )

    def pass_on(prompt, way, hop, q, s):
        final = near_end[way] if hop else jnp.logical_and(near_end[way], prompt == me)

        @pl.when(jnp.logical_and(inner[way], final))
        def _():
            along(prompt, way, hop, q, s, True).start()

        @pl.when(jnp.logical_and(inner[way], jnp.logical_not(final)))
        def _():
            along(prompt, way, hop, q, s).start()

    def across(prompt, s):
        return pltpu.make_async_remote_copy(
            src_ref=box.at[slot(prompt), pieces[s]], dst_ref=box.at[me, pieces[s]],
            send_sem=csend.at[prompt, s], recv_sem=crecv.at[me, s],
            device_id={"sp": prompt}, device_id_type=MESH,
        )

    def normed(latent):
        return (
            latent
            * lax.rsqrt(jnp.mean(latent * latent, axis=-1, keepdims=True) + norm_epsilon)
            * gain_v[...]
        ).astype(BF16)

    def send(group):
        for s in halves[group]:
            for q in range(seq_local):
                prompt = here * seq_local + q
                for way in (0, 1):
                    pass_on(prompt, way, 0, q, s)

                @pl.when(prompt != me)
                def _(s=s):
                    across(prompt, s).start()

    sums = [None] * seq_local
    for n in range(parts):
        for load in firsts[n]:
            load.wait()
        for q in range(seq_local):
            term = jnp.dot(
                tok_v[q, 0:half_rows, n * deep:(n + 1) * deep], kvd_v[n * deep:(n + 1) * deep, :],
                preferred_element_type=F32,
            )
            sums[q] = term if n == 0 else sums[q] + term
    loads[0].wait()
    for q in range(seq_local):
        box[slot(here * seq_local + q), 0:half_rows, :] = normed(sums[q])
    neighbours = jnp.where(here < last, 1, 0) + jnp.where(here > 0, 1, 0)
    pl.semaphore_wait(barrier, sp_count - 1 + sp_count * neighbours)
    send(0)

    for n in (1, 2, 3):
        loads[n].wait()
    for q in range(seq_local):
        mine = slot(here * seq_local + q)
        latent = jnp.dot(tok_v[q, half_rows:pos_dev, :], kvd_v[...], preferred_element_type=F32)
        box[mine, starts[1]:starts[1] + half_rows, :] = normed(latent)
        raw = lax.dot_general(rpt_v[...], tok_v[q], (((1,), (1,)), ((), ())), preferred_element_type=F32)
        cosine, sine_part = tab_v[0], tab_v[1]
        front, back = raw[:half], raw[half:]
        turned = jnp.concatenate(
            [front * cosine - back * sine_part, front * sine_part + back * cosine], axis=0
        ).astype(BF16)
        box[mine, half_rows:half_rows + rope_rows, :] = jnp.concatenate(
            [turned[g * rope_rows:(g + 1) * rope_rows] for g in range(rope_packs)], axis=1
        )
    send(1)

    for n in (4, 5):
        loads[n].wait()
    depth = up_v.shape[1]
    for n, target in enumerate((kw, vw)):
        wide[...] = up_v[n].astype(F32).reshape(depth * tile, key_width)
        for h in range(heads_dev):
            target[:, h * key_width:(h + 1) * key_width] = wide[
                pl.ds(head_off + h, depth, stride=tile), :
            ].astype(BF16)

    for hop in range(last):
        for s in range(count):
            for q in range(seq_local):
                for way in (1, 0):
                    owner = here - 1 - hop if way == 0 else here + 1 + hop
                    prompt = owner * seq_local + q
                    has = owner >= 0 if way == 0 else owner <= last
                    landed = ends[way] if hop else jnp.logical_and(ends[way], prompt == me)

                    @pl.when(jnp.logical_and(has, jnp.logical_not(landed)))
                    def _(way=way, prompt=prompt):
                        along(prompt, way, hop, q, s).wait_recv()
                        if hop + 1 < last:
                            pass_on(prompt, way, hop + 1, q, s)

                        @pl.when(prompt != me)
                        def _():
                            across(prompt, s).start()

    def arrived(source, s):
        part = box.at[source, pieces[s]]
        pltpu.make_async_remote_copy(
            src_ref=part, dst_ref=part,
            send_sem=csend.at[source, s], recv_sem=crecv.at[source, s],
            device_id={"sp": source}, device_id_type=MESH,
        ).wait_recv()

    home = me // seq_local == here
    for group in range(2):
        for step in range(sp_count):
            source = lax.rem(me + step, sp_count)
            for s in halves[group]:
                if step:
                    arrived(source, s)
                else:
                    @pl.when(jnp.logical_and(at_end, jnp.logical_not(home)))
                    def _(s=s):
                        arrived(me, s)
            if group == 1:
                block = pl.ds(pl.multiple_of(source * pos_dev, pos_dev), pos_dev)
                packed = box[source, half_rows:half_rows + rope_rows, :]
                rope_out[0, :, block] = jnp.concatenate(
                    [packed[:, g * pos_dev:(g + 1) * pos_dev] for g in range(rope_packs)], axis=0
                )
            rows = box[source, starts[group]:starts[group] + half_rows, :]
            place = pl.ds(pl.multiple_of(source * pos_dev + group * half_rows, half_rows), half_rows)
            keys = jnp.dot(rows, kw[...], preferred_element_type=F32).astype(BF16)
            values = jnp.dot(rows, vw[...], preferred_element_type=F32).astype(BF16)
            for h in range(heads_dev):
                key_out[0, h, place, :] = keys[:, h * key_width:(h + 1) * key_width]
                val_out[0, h, place, :] = values[:, h * key_width:(h + 1) * key_width]

    for hop in range(last):
        for q in range(seq_local):
            for s in range(count):
                for way in (0, 1):
                    owner = here - hop if way == 0 else here + hop
                    has = owner >= 0 if way == 0 else owner <= last

                    @pl.when(jnp.logical_and(has, inner[way]))
                    def _(way=way, s=s, owner=owner):
                        along(owner * seq_local + q, way, hop, q, s).wait_send()
    for step in range(1, sp_count):
        prompt = lax.rem(me + step, sp_count)
        far = jnp.abs(prompt // seq_local - here) > 1

        @pl.when(jnp.logical_not(jnp.logical_and(at_end, far)))
        def _(prompt=prompt):
            for s in range(count):
                across(prompt, s).wait_send()


def finish(scale, keys, vals, ropes, query, ask, qtab, key_out, val_out, rope_out, read_out, sem):
    heads_dev, key_width = query.shape[1], query.shape[2]
    moves = [pltpu.make_async_copy(ropes, rope_out, sem.at[2, 0])]
    for n, (src, dst) in enumerate([(keys, key_out), (vals, val_out)]):
        for h in range(heads_dev):
            moves.append(pltpu.make_async_copy(src.at[:, h], dst.at[:, h], sem.at[n, h]))
    for move in moves:
        move.start()
    half = ask.shape[2] // 2
    turn = ask[0].astype(F32)
    swapped = jnp.concatenate([-turn[:, half:], turn[:, :half]], axis=1)
    rotated = (turn * qtab[0:1, :] + swapped * qtab[1:2, :]).astype(BF16)
    shape = (heads_dev, heads_dev * key_width)
    own = lax.broadcasted_iota(jnp.int32, shape, 1) // key_width == lax.broadcasted_iota(jnp.int32, shape, 0)
    spread = jnp.where(own, jnp.concatenate([query[0].astype(F32)] * heads_dev, axis=1), 0.0).astype(BF16)
    all_keys = jnp.concatenate([keys[0, h] for h in range(heads_dev)], axis=1)
    total = lax.dot_general(spread, all_keys, (((1,), (1,)), ((), ())), preferred_element_type=F32)
    total = (total + jnp.dot(rotated, ropes[0], preferred_element_type=F32)) * scale
    terms = jnp.exp(total - jnp.max(total, axis=-1, keepdims=True))
    weights = terms / jnp.sum(terms, axis=-1, keepdims=True)
    high = weights.astype(BF16).astype(F32)
    both = jnp.concatenate([high, weights - high], axis=0).astype(BF16)
    all_vals = jnp.concatenate([vals[0, h] for h in range(heads_dev)], axis=1)
    reads = jnp.dot(both, all_vals, preferred_element_type=F32)
    picks = []
    for h in range(heads_dev):
        span = slice(h * key_width, (h + 1) * key_width)
        picks.append(reads[h:h + 1, span] + reads[heads_dev + h:heads_dev + h + 1, span])
    read_out[0] = jnp.concatenate(picks, axis=0).astype(BF16)
    for move in moves:
        move.wait()


def local(tokens, kv_down, rope_down, kv_gain, key_up, value_up, query_nope, query_rope):
    seq_local, pos_dev, model_width = tokens.shape
    sp_count = lax.axis_size("sp")
    tp_count = lax.axis_size("tp")
    latent_width = kv_down.shape[1]
    rope_width = rope_down.shape[1]
    head_count, key_width = key_up.shape[1], key_up.shape[2]
    heads_dev = head_count // tp_count
    length = pos_dev * sp_count
    rope_rows = rope_width * pos_dev // latent_width
    rows = rope_rows + pos_dev
    quarter = pos_dev // 4
    cuts = (0, quarter, 2 * quarter, 3 * quarter + rope_rows, rows)
    parts = 4
    prompts = tp_count * seq_local
    cached, asked = tables(length, rope_width)
    tile = 8
    any_space = pl.BlockSpec(memory_space=pl.ANY)
    hbm = pl.BlockSpec(memory_space=pltpu.HBM)
    vmem = pl.BlockSpec(memory_space=pltpu.VMEM)
    hops = max(tp_count - 1, 1)
    count = len(cuts) - 1
    dma = pltpu.SemaphoreType.DMA
    made = pl.pallas_call(
        functools.partial(kernel, sp_count, tp_count, heads_dev, cuts, parts),
        out_shape=(
            jax.ShapeDtypeStruct((1, heads_dev, length, key_width), BF16),
            jax.ShapeDtypeStruct((1, heads_dev, length, key_width), BF16),
            jax.ShapeDtypeStruct((1, rope_width, length), BF16),
        ),
        in_specs=[hbm] * 7,
        out_specs=(vmem,) * 3,
        scratch_shapes=[
            pltpu.VMEM((sp_count + prompts, rows, latent_width), BF16),
            pltpu.VMEM(tokens.shape, BF16),
            pltpu.VMEM(kv_down.shape, BF16),
            pltpu.VMEM((rope_width, model_width), BF16),
            pltpu.VMEM((1, latent_width), F32),
            pltpu.VMEM((2, latent_width, tile, key_width), BF16),
            pltpu.VMEM((latent_width * tile, key_width), F32),
            pltpu.VMEM((latent_width, heads_dev * key_width), BF16),
            pltpu.VMEM((latent_width, heads_dev * key_width), BF16),
            pltpu.VMEM((2, rope_width // 2, pos_dev), F32),
            dma((parts, 2)),
            dma((6,)),
            dma((2, hops, seq_local, count)),
            dma((2, hops, seq_local, count)),
            dma((prompts, count)),
            dma((sp_count, count)),
        ],
        compiler_params=pltpu.CompilerParams(
            collective_id=0, has_side_effects=True, vmem_limit_bytes=53000000
        ),
    )(
        *[
            pltpu.with_memory_space_constraint(array, pltpu.HBM)
            for array in (
                tokens, kv_down, rope_down.T, kv_gain.reshape(1, latent_width), key_up, value_up,
                jnp.asarray(cached),
            )
        ]
    )
    key_cache, value_cache, rope_t, read_out = pl.pallas_call(
        functools.partial(finish, (key_width + rope_width) ** (-0.5)),
        out_shape=tuple(jax.ShapeDtypeStruct(part.shape, BF16) for part in made)
        + (jax.ShapeDtypeStruct((1, heads_dev, key_width), BF16),),
        in_specs=[vmem] * 6,
        out_specs=(any_space,) * 3 + (vmem,),
        scratch_shapes=[dma((3, heads_dev))],
        compiler_params=pltpu.CompilerParams(vmem_limit_bytes=8 * 1024 * 1024),
    )(*made, query_nope, query_rope, jnp.asarray(asked))
    return (key_cache, value_cache, jnp.swapaxes(rope_t, 1, 2), read_out)


def solution(mesh):
    placed = (
        P(("grp", "tp"), "sp", None),
        P(),
        P(),
        P(),
        P(),
        P(),
        P(("grp", "sp"), "tp", None),
        P(("grp", "sp"), "tp", None),
    )
    return jax.shard_map(
        local,
        mesh=mesh,
        in_specs=placed,
        out_specs=(
            P(("grp", "sp"), "tp", None, None),
            P(("grp", "sp"), "tp", None, None),
            P(("grp", "sp"), None, None),
            P(("grp", "sp"), "tp", None),
        ),
        check_vma=False,
    )
```

time: 35.3 us -> 29 us (0.82)
  Pallas kernels: 31.9 us -> 28.2 us
  local copies, waits for them, and re-layouts: 2.58 us -> 0.02 us
    pallas_call x1, Pallas kernels: 29.7 us -> 25.9 us  [local(): pl.pallas_call(functools.partial(kernel, sp_count, tp_count, heads_dev, c...]
    unnamed x12 -> x6, local copies, waits for them, and re-layouts: 2.58 us -> 0.02 us
where the time goes in v1:
time: 29 us; the launch traced here: 28.9 us
  Pallas kernels  28.2 us (97%)
  between operations  0.69 us (2%)
    pallas_call x1, Pallas kernels, local(): pl.pallas_call(functools.partial(kernel, sp_count, tp_count, heads_dev, c...  25.9 us
    pallas_call x1, Pallas kernels, local(): pl.pallas_call(functools.partial(finish, (key_width + rope_width) ** (-0....  2.25 us

profile of v1, /device:TPU:5, one launch (start us, length us, event | category | flops | bytes accessed | tf_op | source)
XLA Modules:
  0.0 28.9 jit_solution(15410163753143229916)
XLA Ops:
  0.6 0.0 copy-start
  0.6 0.0 copy-start.1
  0.7 0.0 copy-start.2
  0.7 25.9 %shard_map.129 = (bf16[1,4,1024,128]{3,2,1,0:T(8,128)(2,1)S(1)}, bf16[1,4,1024,128]{3,2,1,0:T(8,128)(2,1)S(1)}, bf16[1,64,1024]{2,1,0:T(8,128)(2,1)S(1)}) custom-call(bf16[1,256,2048]{2,1,0:T(8,128)(2,1)} %tok.1, bf16[2048,512]{1,0:T(8,128)(2,1)} %kvd.1, bf16[64,2048]{1,0:T(8,128)(2,1)} %bitcast.3, f32[1,512]{1,0:T(1,128)} %bitcast.4, ...), custom_call_target="tpu_custom_call" | custom-call | tf_op jit(solution)/shard_map/pallas_call | solution.py:326
  26.6 0.0 copy-done
  26.6 0.0 copy-done.1
  26.6 0.0 copy-done.2
  26.6 2.2 %shard_map.130 = (bf16[1,4,1024,128]{3,2,1,0:T(8,128)(2,1)}, bf16[1,4,1024,128]{3,2,1,0:T(8,128)(2,1)}, bf16[1,64,1024]{2,1,0:T(8,128)(2,1)}, bf16[1,4,128]{2,1,0:T(4,128)(2,1)}) custom-call(bf16[1,4,1024,128]{3,2,1,0:T(8,128)(2,1)S(1)} %get-tuple-element.11.keys, bf16[1,4,1024,128]{3,2,1,0:T(8,128)(2,1)S(1)} %get-tuple-element.12.vals, ...), custom_call_target="tpu_custom_call" | custom-call | tf_op jit(solution)/shard_map/pallas_call | solution.py:365
Async XLA Ops:
  0.6 26.0 %copy-start = (bf16[1,4,128]{2,1,0:T(4,128)(2,1)S(1)}, bf16[1,4,128]{2,1,0:T(4,128)(2,1)}, u32[]{:S(2)}) copy-start(bf16[1,4,128]{2,1,0:T(4,128)(2,1)} %query.1) | copy-start | bytes 3076
  0.6 26.0 %copy-start.1 = (bf16[1,4,64]{2,1,0:T(4,128)(2,1)S(1)}, bf16[1,4,64]{2,1,0:T(4,128)(2,1)}, u32[]{:S(2)}) copy-start(bf16[1,4,64]{2,1,0:T(4,128)(2,1)} %ask.1) | copy-start | bytes 1540
  0.7 26.0 %copy-start.2 = (f32[2,64]{1,0:T(2,128)S(1)}, f32[2,64]{1,0:T(2,128)}, u32[]{:S(2)}) copy-start(f32[2,64]{1,0:T(2,128)} %constant.5.clone.qtab) | copy-start | bytes 1540

commit v2 on v1

--- a/solution.py
+++ b/solution.py
@@ -24,11 +24,11 @@
 
 
 def kernel(
-    sp_count, tp_count, heads_dev, cuts, parts,
+    sp_count, tp_count, heads_dev, cuts, groups, parts,
     tok, kvd, rpt, gain, kup, vup, tab,
     key_out, val_out, rope_out,
     box, tok_v, kvd_v, rpt_v, gain_v, up_v, wide, kw, vw, tab_v,
-    first_sem, in_sem, zsend, zrecv, csend, crecv,
+    first_sem, in_sem, sent, zrecv, crecv,
 ):
     me = lax.axis_index("sp")
     here = lax.axis_index("tp")
@@ -47,23 +47,9 @@
     at_end = jnp.logical_or(here == 0, here == last)
 
     half_rows = pos_dev // 2
-    starts = (0, half_rows + rope_rows)
     halves = ([s for s in range(count) if cuts[s] < half_rows], [s for s in range(count) if cuts[s] >= half_rows])
-
-    barrier = pltpu.get_barrier_semaphore()
-    for step in range(1, sp_count):
-        pl.semaphore_signal(
-            barrier, inc=1, device_id={"sp": lax.rem(me + step, sp_count)}, device_id_type=MESH
-        )
-    for way in (0, 1):
-        @pl.when(inner[way])
-        def _(way=way):
-            for step in range(sp_count):
-                pl.semaphore_signal(
-                    barrier, inc=1,
-                    device_id={"sp": lax.rem(me + step, sp_count), "tp": here + (1 if way == 0 else -1)},
-                    device_id_type=MESH,
-                )
+    spans = [pl.ds(cuts[g[0]], cuts[g[-1] + 1] - cuts[g[0]]) for g in groups]
+    group_of = {s: n for n, g in enumerate(groups) for s in g}
 
     tile = up_v.shape[2]
     head_start = here * heads_dev
@@ -90,46 +76,75 @@
             (tok.at[:, half_rows:pos_dev, :], tok_v.at[:, half_rows:pos_dev, :]),
             (rpt, rpt_v),
             (tab.at[:, :, pl.ds(pl.multiple_of(me * pos_dev, pos_dev), pos_dev)], tab_v),
-            (kup.at[:, pl.ds(head_tile, tile), :], up_v.at[0]),
-            (vup.at[:, pl.ds(head_tile, tile), :], up_v.at[1]),
         ])
     ]
-    for load in loads:
+    ups = [
+        pltpu.make_async_copy(src.at[:, pl.ds(head_tile, tile), :], up_v.at[n], in_sem.at[4])
+        for n, src in enumerate((kup, vup))
+    ]
+    for load in loads + ups:
         load.start()
+
+    barrier = pltpu.get_barrier_semaphore()
+    for way in (0, 1):
+        @pl.when(inner[way])
+        def _(way=way):
+            pl.semaphore_signal(
+                barrier, inc=1, device_id={"tp": here + (1 if way == 0 else -1)}, device_id_type=MESH
+            )
+    for step in range(1, sp_count):
+        pl.semaphore_signal(
+            barrier, inc=1, device_id={"sp": lax.rem(me + step, sp_count)}, device_id_type=MESH
+        )
+    for way in (0, 1):
+        @pl.when(jnp.logical_and(ends[way], inner[1 - way]))
+        def _(way=way):
+            for step in range(1, sp_count):
+                pl.semaphore_signal(
+                    barrier, inc=1,
+                    device_id={"sp": lax.rem(me + step, sp_count), "tp": here + (-1 if way == 0 else 1)},
+                    device_id_type=MESH,
+                )
+
+    def greeted():
+        total = sp_count - 1
+        for way in (0, 1):
+            total = total + jnp.where(inner[way], jnp.where(near_end[way], sp_count, 1), 0)
+        pl.semaphore_wait(barrier, total)
 
     def slot(prompt):
         return jnp.where(prompt == me, me, sp_count + prompt)
 
-    def along(prompt, way, hop, q, s, final=False):
+    def along(prompt, way, s, final=False):
         part = box.at[slot(prompt), pieces[s]]
         tp = here + (1 if way == 0 else -1)
         if final:
             return pltpu.make_async_remote_copy(
                 src_ref=part, dst_ref=box.at[me, pieces[s]],
-                send_sem=zsend.at[way, hop, q, s], recv_sem=crecv.at[me, s],
+                send_sem=sent.at[0], recv_sem=crecv.at[me, group_of[s]],
                 device_id={"sp": prompt, "tp": tp}, device_id_type=MESH,
             )
         return pltpu.make_async_remote_copy(
             src_ref=part, dst_ref=part,
-            send_sem=zsend.at[way, hop, q, s], recv_sem=zrecv.at[way, hop, q, s],
+            send_sem=sent.at[0], recv_sem=zrecv.at[prompt, s],
             device_id={"sp": me, "tp": tp}, device_id_type=MESH,
         )
 
-    def pass_on(prompt, way, hop, q, s):
+    def pass_on(prompt, way, hop, s):
         final = near_end[way] if hop else jnp.logical_and(near_end[way], prompt == me)
 
         @pl.when(jnp.logical_and(inner[way], final))
         def _():
-            along(prompt, way, hop, q, s, True).start()
+            along(prompt, way, s, True).start()
 
         @pl.when(jnp.logical_and(inner[way], jnp.logical_not(final)))
         def _():
-            along(prompt, way, hop, q, s).start()
+            along(prompt, way, s).start()
 
     def across(prompt, s):
         return pltpu.make_async_remote_copy(
             src_ref=box.at[slot(prompt), pieces[s]], dst_ref=box.at[me, pieces[s]],
-            send_sem=csend.at[prompt, s], recv_sem=crecv.at[me, s],
+            send_sem=sent.at[1], recv_sem=crecv.at[me, group_of[s]],
             device_id={"sp": prompt}, device_id_type=MESH,
         )
 
@@ -145,7 +160,7 @@
             for q in range(seq_local):
                 prompt = here * seq_local + q
                 for way in (0, 1):
-                    pass_on(prompt, way, 0, q, s)
+                    pass_on(prompt, way, 0, s)
 
                 @pl.when(prompt != me)
                 def _(s=s):
@@ -164,8 +179,7 @@
     loads[0].wait()
     for q in range(seq_local):
         box[slot(here * seq_local + q), 0:half_rows, :] = normed(sums[q])
-    neighbours = jnp.where(here < last, 1, 0) + jnp.where(here > 0, 1, 0)
-    pl.semaphore_wait(barrier, sp_count - 1 + sp_count * neighbours)
+    greeted()
     send(0)
 
     for n in (1, 2, 3):
@@ -173,7 +187,7 @@
     for q in range(seq_local):
         mine = slot(here * seq_local + q)
         latent = jnp.dot(tok_v[q, half_rows:pos_dev, :], kvd_v[...], preferred_element_type=F32)
-        box[mine, starts[1]:starts[1] + half_rows, :] = normed(latent)
+        box[mine, half_rows + rope_rows:pos_dev + rope_rows, :] = normed(latent)
         raw = lax.dot_general(rpt_v[...], tok_v[q], (((1,), (1,)), ((), ())), preferred_element_type=F32)
         cosine, sine_part = tab_v[0], tab_v[1]
         front, back = raw[:half], raw[half:]
@@ -185,8 +199,7 @@
         )
     send(1)
 
-    for n in (4, 5):
-        loads[n].wait()
+    pltpu.make_async_copy(up_v, up_v, in_sem.at[4]).wait()
     depth = up_v.shape[1]
     for n, target in enumerate((kw, vw)):
         wide[...] = up_v[n].astype(F32).reshape(depth * tile, key_width)
@@ -206,73 +219,81 @@
 
                     @pl.when(jnp.logical_and(has, jnp.logical_not(landed)))
                     def _(way=way, prompt=prompt):
-                        along(prompt, way, hop, q, s).wait_recv()
+                        along(prompt, way, s).wait_recv()
                         if hop + 1 < last:
-                            pass_on(prompt, way, hop + 1, q, s)
+                            pass_on(prompt, way, hop + 1, s)
 
                         @pl.when(prompt != me)
                         def _():
                             across(prompt, s).start()
 
-    def arrived(source, s):
-        part = box.at[source, pieces[s]]
+    def arrived(source, group):
+        part = box.at[source, spans[group]]
         pltpu.make_async_remote_copy(
-            src_ref=part, dst_ref=part,
-            send_sem=csend.at[source, s], recv_sem=crecv.at[source, s],
+            src_ref=part, dst_ref=part, send_sem=sent.at[1], recv_sem=crecv.at[source, group],
             device_id={"sp": source}, device_id_type=MESH,
         ).wait_recv()
 
     home = me // seq_local == here
-    for group in range(2):
-        for step in range(sp_count):
-            source = lax.rem(me + step, sp_count)
-            for s in halves[group]:
+    for group, members in enumerate(groups):
+        begin, stop = cuts[members[0]], cuts[members[-1] + 1]
+        with_rope = begin <= half_rows < stop
+        if with_rope:
+            begin = begin + rope_rows
+        height = stop - begin
+        first = begin if begin < half_rows else begin - rope_rows
+        batch = max(pos_dev // height, 1)
+        for base in range(0, sp_count, batch):
+            steps = range(base, min(base + batch, sp_count))
+            sources = [lax.rem(me + step, sp_count) for step in steps]
+            for step, source in zip(steps, sources):
                 if step:
-                    arrived(source, s)
+                    arrived(source, group)
                 else:
                     @pl.when(jnp.logical_and(at_end, jnp.logical_not(home)))
-                    def _(s=s):
-                        arrived(me, s)
-            if group == 1:
-                block = pl.ds(pl.multiple_of(source * pos_dev, pos_dev), pos_dev)
-                packed = box[source, half_rows:half_rows + rope_rows, :]
-                rope_out[0, :, block] = jnp.concatenate(
-                    [packed[:, g * pos_dev:(g + 1) * pos_dev] for g in range(rope_packs)], axis=0
-                )
-            rows = box[source, starts[group]:starts[group] + half_rows, :]
-            place = pl.ds(pl.multiple_of(source * pos_dev + group * half_rows, half_rows), half_rows)
-            keys = jnp.dot(rows, kw[...], preferred_element_type=F32).astype(BF16)
-            values = jnp.dot(rows, vw[...], preferred_element_type=F32).astype(BF16)
-            for h in range(heads_dev):
-                key_out[0, h, place, :] = keys[:, h * key_width:(h + 1) * key_width]
-                val_out[0, h, place, :] = values[:, h * key_width:(h + 1) * key_width]
-
-    for hop in range(last):
-        for q in range(seq_local):
-            for s in range(count):
-                for way in (0, 1):
-                    owner = here - hop if way == 0 else here + hop
-                    has = owner >= 0 if way == 0 else owner <= last
-
-                    @pl.when(jnp.logical_and(has, inner[way]))
-                    def _(way=way, s=s, owner=owner):
-                        along(owner * seq_local + q, way, hop, q, s).wait_send()
-    for step in range(1, sp_count):
-        prompt = lax.rem(me + step, sp_count)
-        far = jnp.abs(prompt // seq_local - here) > 1
-
-        @pl.when(jnp.logical_not(jnp.logical_and(at_end, far)))
-        def _(prompt=prompt):
-            for s in range(count):
-                across(prompt, s).wait_send()
-
-
-def finish(scale, keys, vals, ropes, query, ask, qtab, key_out, val_out, rope_out, read_out, sem):
+                    def _():
+                        arrived(me, group)
+                if with_rope:
+                    block = pl.ds(pl.multiple_of(source * pos_dev, pos_dev), pos_dev)
+                    packed = box[source, half_rows:half_rows + rope_rows, :]
+                    rope_out[0, :, block] = jnp.concatenate(
+                        [packed[:, g * pos_dev:(g + 1) * pos_dev] for g in range(rope_packs)], axis=0
+                    )
+            rows = jnp.concatenate([box[source, begin:stop, :] for source in sources], axis=0)
+            for weight, target in ((kw, key_out), (vw, val_out)):
+                made = jnp.dot(rows, weight[...], preferred_element_type=F32).astype(BF16)
+                for n, source in enumerate(sources):
+                    place = pl.ds(pl.multiple_of(source * pos_dev + first, height), height)
+                    for h in range(heads_dev):
+                        target[0, h, place, :] = made[
+                            n * height:(n + 1) * height, h * key_width:(h + 1) * key_width
+                        ]
+
+    def drain(index, blocks, most):
+        for n in range(1, most + 1):
+            @pl.when(blocks == n)
+            def _(n=n):
+                part = box.at[0:n]
+                pltpu.make_async_remote_copy(
+                    src_ref=part, dst_ref=part, send_sem=sent.at[index], recv_sem=crecv.at[0, 0],
+                    device_id={"sp": me}, device_id_type=MESH,
+                ).wait_send()
+
+    upward = jnp.where(inner[0], (here + 1) * seq_local, 0)
+    downward = jnp.where(inner[1], (tp_count - here) * seq_local, 0)
+    drain(0, upward + downward, (tp_count + 1) * seq_local if tp_count > 1 else 0)
+    prompts = tp_count * seq_local
+    beside = jnp.logical_or(jnp.logical_not(at_end), jnp.abs(me // seq_local - here) <= 1)
+    reach = jnp.where(at_end, min(tp_count, 2) * seq_local, prompts)
+    drain(1, reach - jnp.where(beside, 1, 0), prompts)
+
+
+def finish(scale, keys, vals, ropes, query, ask, qtab, key_out, val_out, rope_out, read_out, read, sem):
     heads_dev, key_width = query.shape[1], query.shape[2]
-    moves = [pltpu.make_async_copy(ropes, rope_out, sem.at[2, 0])]
-    for n, (src, dst) in enumerate([(keys, key_out), (vals, val_out)]):
-        for h in range(heads_dev):
-            moves.append(pltpu.make_async_copy(src.at[:, h], dst.at[:, h], sem.at[n, h]))
+    moves = [
+        pltpu.make_async_copy(src, dst, sem.at[n])
+        for n, (src, dst) in enumerate([(keys, key_out), (vals, val_out), (ropes, rope_out)])
+    ]
     for move in moves:
         move.start()
     half = ask.shape[2] // 2
@@ -295,7 +316,9 @@
     for h in range(heads_dev):
         span = slice(h * key_width, (h + 1) * key_width)
         picks.append(reads[h:h + 1, span] + reads[heads_dev + h:heads_dev + h + 1, span])
-    read_out[0] = jnp.concatenate(picks, axis=0).astype(BF16)
+    read[0] = jnp.concatenate(picks, axis=0).astype(BF16)
+    moves.append(pltpu.make_async_copy(read, read_out, sem.at[3]))
+    moves[-1].start()
     for move in moves:
         move.wait()
 
@@ -313,6 +336,7 @@
     rows = rope_rows + pos_dev
     quarter = pos_dev // 4
     cuts = (0, quarter, 2 * quarter, 3 * quarter + rope_rows, rows)
+    groups = ((0, 1), (2,), (3,))
     parts = 4
     prompts = tp_count * seq_local
     cached, asked = tables(length, rope_width)
@@ -320,11 +344,10 @@
     any_space = pl.BlockSpec(memory_space=pl.ANY)
     hbm = pl.BlockSpec(memory_space=pltpu.HBM)
     vmem = pl.BlockSpec(memory_space=pltpu.VMEM)
-    hops = max(tp_count - 1, 1)
     count = len(cuts) - 1
     dma = pltpu.SemaphoreType.DMA
     made = pl.pallas_call(
-        functools.partial(kernel, sp_count, tp_count, heads_dev, cuts, parts),
+        functools.partial(kernel, sp_count, tp_count, heads_dev, cuts, groups, parts),
         out_shape=(
             jax.ShapeDtypeStruct((1, heads_dev, length, key_width), BF16),
             jax.ShapeDtypeStruct((1, heads_dev, length, key_width), BF16),
@@ -344,11 +367,10 @@
             pltpu.VMEM((latent_width, heads_dev * key_width), BF16),
             pltpu.VMEM((2, rope_width // 2, pos_dev), F32),
             dma((parts, 2)),
-            dma((6,)),
-            dma((2, hops, seq_local, count)),
-            dma((2, hops, seq_local, count)),
+            dma((5,)),
+            dma((2,)),
             dma((prompts, count)),
-            dma((sp_count, count)),
+            dma((sp_count, len(groups))),
         ],
         compiler_params=pltpu.CompilerParams(
             collective_id=0, has_side_effects=True, vmem_limit_bytes=53000000
@@ -367,8 +389,8 @@
         out_shape=tuple(jax.ShapeDtypeStruct(part.shape, BF16) for part in made)
         + (jax.ShapeDtypeStruct((1, heads_dev, key_width), BF16),),
         in_specs=[vmem] * 6,
-        out_specs=(any_space,) * 3 + (vmem,),
-        scratch_shapes=[dma((3, heads_dev))],
+        out_specs=(any_space,) * 4,
+        scratch_shapes=[pltpu.VMEM((1, heads_dev, key_width), BF16), dma((4,))],
         compiler_params=pltpu.CompilerParams(vmem_limit_bytes=8 * 1024 * 1024),
     )(*made, query_nope, query_rope, jnp.asarray(asked))
     return (key_cache, value_cache, jnp.swapaxes(rope_t, 1, 2), read_out)

time: 29 us -> 26.4 us (0.910)
  Pallas kernels: 28.2 us -> 25.6 us
    pallas_call x1, Pallas kernels: 25.9 us -> 24.1 us  [local(): pl.pallas_call(functools.partial(kernel, sp_count, tp_count, heads_dev, c...]
    pallas_call x1, Pallas kernels: 2.25 us -> 1.48 us  [local(): pl.pallas_call(functools.partial(finish, (key_width + rope_width) ** (-0....]
where the time goes in v2:
time: 26.4 us; the launch traced here: 26.3 us
  Pallas kernels  25.6 us (97%)
  between operations  0.69 us (3%)
    pallas_call x1, Pallas kernels, local(): pl.pallas_call(functools.partial(kernel, sp_count, tp_count, heads_dev, c...  24.1 us
    pallas_call x1, Pallas kernels, local(): pl.pallas_call(functools.partial(finish, (key_width + rope_width) ** (-0....  1.48 us

profile of v2, /device:TPU:5, one launch (start us, length us, event | category | flops | bytes accessed | tf_op | source)
XLA Modules:
  0.0 26.3 jit_solution(8400939090772686661)
XLA Ops:
  0.6 0.0 copy-start
  0.6 0.0 copy-start.1
  0.7 0.0 copy-start.2
  0.7 24.1 %shard_map.129 = (bf16[1,4,1024,128]{3,2,1,0:T(8,128)(2,1)S(1)}, bf16[1,4,1024,128]{3,2,1,0:T(8,128)(2,1)S(1)}, bf16[1,64,1024]{2,1,0:T(8,128)(2,1)S(1)}) custom-call(bf16[1,256,2048]{2,1,0:T(8,128)(2,1)} %tok.1, bf16[2048,512]{1,0:T(8,128)(2,1)} %kvd.1, bf16[64,2048]{1,0:T(8,128)(2,1)} %bitcast.3, f32[1,512]{1,0:T(1,128)} %bitcast.4, ...), custom_call_target="tpu_custom_call" | custom-call | tf_op jit(solution)/shard_map/pallas_call | solution.py:349
  24.8 0.0 copy-done
  24.8 0.0 copy-done.1
  24.8 0.0 copy-done.2
  24.8 1.5 %shard_map.130 = (bf16[1,4,1024,128]{3,2,1,0:T(8,128)(2,1)}, bf16[1,4,1024,128]{3,2,1,0:T(8,128)(2,1)}, bf16[1,64,1024]{2,1,0:T(8,128)(2,1)}, bf16[1,4,128]{2,1,0:T(4,128)(2,1)}) custom-call(bf16[1,4,1024,128]{3,2,1,0:T(8,128)(2,1)S(1)} %get-tuple-element.11.keys, bf16[1,4,1024,128]{3,2,1,0:T(8,128)(2,1)S(1)} %get-tuple-element.12.vals, ...), custom_call_target="tpu_custom_call" | custom-call | tf_op jit(solution)/shard_map/pallas_call | solution.py:387
Async XLA Ops:
  0.6 24.1 %copy-start = (bf16[1,4,128]{2,1,0:T(4,128)(2,1)S(1)}, bf16[1,4,128]{2,1,0:T(4,128)(2,1)}, u32[]{:S(2)}) copy-start(bf16[1,4,128]{2,1,0:T(4,128)(2,1)} %query.1) | copy-start | bytes 3076
  0.6 24.1 %copy-start.1 = (bf16[1,4,64]{2,1,0:T(4,128)(2,1)S(1)}, bf16[1,4,64]{2,1,0:T(4,128)(2,1)}, u32[]{:S(2)}) copy-start(bf16[1,4,64]{2,1,0:T(4,128)(2,1)} %ask.1) | copy-start | bytes 1540
  0.7 24.1 %copy-start.2 = (f32[2,64]{1,0:T(2,128)S(1)}, f32[2,64]{1,0:T(2,128)}, u32[]{:S(2)}) copy-start(f32[2,64]{1,0:T(2,128)} %constant.5.clone.qtab) | copy-start | bytes 1540

commit v3 on v2

--- a/solution.py
+++ b/solution.py
@@ -24,15 +24,16 @@
 
 
 def kernel(
-    sp_count, tp_count, heads_dev, cuts, groups, parts,
+    sp_count, tp_count, heads_dev, lead, rope_at, cuts, groups, parts,
     tok, kvd, rpt, gain, kup, vup, tab,
     key_out, val_out, rope_out,
     box, tok_v, kvd_v, rpt_v, gain_v, up_v, wide, kw, vw, tab_v,
-    first_sem, in_sem, sent, zrecv, crecv,
+    load_sem, sent, zrecv, crecv, ready,
 ):
     me = lax.axis_index("sp")
     here = lax.axis_index("tp")
     seq_local, pos_dev, model_width = tok.shape
+    latent_width = kvd.shape[1]
     rope_width = rpt.shape[0]
     half = rope_width // 2
     key_width = kup.shape[2]
@@ -41,13 +42,12 @@
     pieces = [pl.ds(a, b - a) for a, b in zip(cuts[:-1], cuts[1:])]
     count = len(pieces)
     last = tp_count - 1
+    prompts = tp_count * seq_local
     inner = {0: here < last, 1: here > 0}
     ends = {0: here == last, 1: here == 0}
     near_end = {0: here + 1 == last, 1: here - 1 == 0}
     at_end = jnp.logical_or(here == 0, here == last)
 
-    half_rows = pos_dev // 2
-    halves = ([s for s in range(count) if cuts[s] < half_rows], [s for s in range(count) if cuts[s] >= half_rows])
     spans = [pl.ds(cuts[g[0]], cuts[g[-1] + 1] - cuts[g[0]]) for g in groups]
     group_of = {s: n for n, g in enumerate(groups) for s in g}
 
@@ -56,35 +56,36 @@
     head_tile = pl.multiple_of(head_start // tile * tile, tile)
     head_off = lax.rem(head_start, tile)
     deep = model_width // parts
+
+    def load(pairs, index):
+        size = 0
+        for src, dst in pairs:
+            pltpu.make_async_copy(src, dst, load_sem.at[index]).start()
+            size += int(np.prod(dst.shape)) * dst.dtype.itemsize
+        rows = size // (latent_width * kvd_v.dtype.itemsize)
+        whole = kvd_v.at[0:rows, :]
+        return pltpu.make_async_copy(whole, whole, load_sem.at[index])
+
     firsts = []
     for n in range(parts):
         span = pl.ds(n * deep, deep)
-        firsts.append([
-            pltpu.make_async_copy(src, dst, first_sem.at[n, m])
-            for m, (src, dst) in enumerate([
-                (kvd.at[span, :], kvd_v.at[span, :]),
-                (tok.at[:, 0:half_rows, span], tok_v.at[:, 0:half_rows, span]),
-            ])
-        ])
-    for pair in firsts:
-        for load in pair:
-            load.start()
-    loads = [
-        pltpu.make_async_copy(src, dst, in_sem.at[n])
-        for n, (src, dst) in enumerate([
-            (gain, gain_v),
-            (tok.at[:, half_rows:pos_dev, :], tok_v.at[:, half_rows:pos_dev, :]),
-            (rpt, rpt_v),
-            (tab.at[:, :, pl.ds(pl.multiple_of(me * pos_dev, pos_dev), pos_dev)], tab_v),
-        ])
-    ]
-    ups = [
-        pltpu.make_async_copy(src.at[:, pl.ds(head_tile, tile), :], up_v.at[n], in_sem.at[4])
-        for n, src in enumerate((kup, vup))
-    ]
-    for load in loads + ups:
-        load.start()
-
+        firsts.append(load([
+            (kvd.at[span, :], kvd_v.at[span, :]),
+            (tok.at[:, 0:lead, span], tok_v.at[:, 0:lead, span]),
+        ], n))
+    gains = pltpu.make_async_copy(gain, gain_v, load_sem.at[parts])
+    gains.start()
+    rest = load([
+        (tok.at[:, lead:pos_dev, :], tok_v.at[:, lead:pos_dev, :]),
+        (rpt, rpt_v),
+        (tab.at[:, :, pl.ds(pl.multiple_of(me * pos_dev, pos_dev), pos_dev)], tab_v),
+    ], parts + 1)
+    for n, src in enumerate((kup, vup)):
+        pltpu.make_async_copy(
+            src.at[:, pl.ds(head_tile, tile), :], up_v.at[n], load_sem.at[parts + 2]
+        ).start()
+
+    lanes = [*range(1, sp_count, 2), *range(0, sp_count, 2)]
     barrier = pltpu.get_barrier_semaphore()
     for way in (0, 1):
         @pl.when(inner[way])
@@ -96,21 +97,6 @@
         pl.semaphore_signal(
             barrier, inc=1, device_id={"sp": lax.rem(me + step, sp_count)}, device_id_type=MESH
         )
-    for way in (0, 1):
-        @pl.when(jnp.logical_and(ends[way], inner[1 - way]))
-        def _(way=way):
-            for step in range(1, sp_count):
-                pl.semaphore_signal(
-                    barrier, inc=1,
-                    device_id={"sp": lax.rem(me + step, sp_count), "tp": here + (-1 if way == 0 else 1)},
-                    device_id_type=MESH,
-                )
-
-    def greeted():
-        total = sp_count - 1
-        for way in (0, 1):
-            total = total + jnp.where(inner[way], jnp.where(near_end[way], sp_count, 1), 0)
-        pl.semaphore_wait(barrier, total)
 
     def slot(prompt):
         return jnp.where(prompt == me, me, sp_count + prompt)
@@ -155,11 +141,11 @@
             * gain_v[...]
         ).astype(BF16)
 
-    def send(group):
-        for s in halves[group]:
+    def send(chosen):
+        for s in chosen:
             for q in range(seq_local):
                 prompt = here * seq_local + q
-                for way in (0, 1):
+                for way in (1, 0):
                     pass_on(prompt, way, 0, s)
 
                 @pl.when(prompt != me)
@@ -168,38 +154,50 @@
 
     sums = [None] * seq_local
     for n in range(parts):
-        for load in firsts[n]:
-            load.wait()
+        firsts[n].wait()
         for q in range(seq_local):
             term = jnp.dot(
-                tok_v[q, 0:half_rows, n * deep:(n + 1) * deep], kvd_v[n * deep:(n + 1) * deep, :],
+                tok_v[q, 0:lead, n * deep:(n + 1) * deep], kvd_v[n * deep:(n + 1) * deep, :],
                 preferred_element_type=F32,
             )
             sums[q] = term if n == 0 else sums[q] + term
-    loads[0].wait()
+    gains.wait()
     for q in range(seq_local):
-        box[slot(here * seq_local + q), 0:half_rows, :] = normed(sums[q])
-    greeted()
-    send(0)
-
-    for n in (1, 2, 3):
-        loads[n].wait()
+        box[slot(here * seq_local + q), 0:lead, :] = normed(sums[q])
+    pl.semaphore_wait(
+        barrier, sp_count - 1 + jnp.where(inner[0], 1, 0) + jnp.where(inner[1], 1, 0)
+    )
+    send((0,))
+
+    for way in (0, 1):
+        @pl.when(jnp.logical_and(ends[way], inner[1 - way]))
+        def _(way=way):
+            pl.semaphore_signal(
+                ready.at[0], inc=1, device_id={"tp": here + (-1 if way == 0 else 1)}, device_id_type=MESH
+            )
+
+    def finish_rows(begin, stop, place):
+        for q in range(seq_local):
+            latent = jnp.dot(tok_v[q, begin:stop, :], kvd_v[...], preferred_element_type=F32)
+            box[slot(here * seq_local + q), place:place + stop - begin, :] = normed(latent)
+
+    rest.wait()
+    finish_rows(lead, rope_at, lead)
+    send((1,))
+    finish_rows(rope_at, pos_dev, rope_at + rope_rows)
     for q in range(seq_local):
-        mine = slot(here * seq_local + q)
-        latent = jnp.dot(tok_v[q, half_rows:pos_dev, :], kvd_v[...], preferred_element_type=F32)
-        box[mine, half_rows + rope_rows:pos_dev + rope_rows, :] = normed(latent)
         raw = lax.dot_general(rpt_v[...], tok_v[q], (((1,), (1,)), ((), ())), preferred_element_type=F32)
         cosine, sine_part = tab_v[0], tab_v[1]
         front, back = raw[:half], raw[half:]
         turned = jnp.concatenate(
             [front * cosine - back * sine_part, front * sine_part + back * cosine], axis=0
         ).astype(BF16)
-        box[mine, half_rows:half_rows + rope_rows, :] = jnp.concatenate(
+        box[slot(here * seq_local + q), rope_at:rope_at + rope_rows, :] = jnp.concatenate(
             [turned[g * rope_rows:(g + 1) * rope_rows] for g in range(rope_packs)], axis=1
         )
-    send(1)
-
-    pltpu.make_async_copy(up_v, up_v, in_sem.at[4]).wait()
+    send(range(2, count))
+
+    pltpu.make_async_copy(up_v, up_v, load_sem.at[parts + 2]).wait()
     depth = up_v.shape[1]
     for n, target in enumerate((kw, vw)):
         wide[...] = up_v[n].astype(F32).reshape(depth * tile, key_width)
@@ -207,6 +205,11 @@
             target[:, h * key_width:(h + 1) * key_width] = wide[
                 pl.ds(head_off + h, depth, stride=tile), :
             ].astype(BF16)
+
+    for way in (0, 1):
+        @pl.when(jnp.logical_and(inner[way], near_end[way]))
+        def _():
+            pl.semaphore_wait(ready.at[0], 1)
 
     for hop in range(last):
         for s in range(count):
@@ -231,39 +234,34 @@
         part = box.at[source, spans[group]]
         pltpu.make_async_remote_copy(
             src_ref=part, dst_ref=part, send_sem=sent.at[1], recv_sem=crecv.at[source, group],
-            device_id={"sp": source}, device_id_type=MESH,
+            device_id={"sp": me}, device_id_type=MESH,
         ).wait_recv()
 
-    home = me // seq_local == here
+    landed = jnp.logical_and(at_end, me // seq_local != here)
     for group, members in enumerate(groups):
         begin, stop = cuts[members[0]], cuts[members[-1] + 1]
-        with_rope = begin <= half_rows < stop
-        if with_rope:
-            begin = begin + rope_rows
-        height = stop - begin
-        first = begin if begin < half_rows else begin - rope_rows
-        batch = max(pos_dev // height, 1)
+        with_rope = begin <= rope_at < stop
+        ranges = [(begin, rope_at), (rope_at + rope_rows, stop)] if with_rope else [(begin, stop)]
+        ranges = [(a, b) for a, b in ranges if b > a]
+        height = sum(b - a for a, b in ranges)
+        first = begin if begin <= rope_at else begin - rope_rows
+        batch = 4 if group == len(groups) - 1 else 2
         for base in range(0, sp_count, batch):
-            steps = range(base, min(base + batch, sp_count))
-            sources = [lax.rem(me + step, sp_count) for step in steps]
-            for step, source in zip(steps, sources):
-                if step:
+            sources = lanes[base:base + batch]
+            for source in sources:
+                @pl.when(jnp.logical_or(me != source, landed))
+                def _(source=source):
                     arrived(source, group)
-                else:
-                    @pl.when(jnp.logical_and(at_end, jnp.logical_not(home)))
-                    def _():
-                        arrived(me, group)
                 if with_rope:
-                    block = pl.ds(pl.multiple_of(source * pos_dev, pos_dev), pos_dev)
-                    packed = box[source, half_rows:half_rows + rope_rows, :]
-                    rope_out[0, :, block] = jnp.concatenate(
+                    packed = box[source, rope_at:rope_at + rope_rows, :]
+                    rope_out[0, :, source * pos_dev:(source + 1) * pos_dev] = jnp.concatenate(
                         [packed[:, g * pos_dev:(g + 1) * pos_dev] for g in range(rope_packs)], axis=0
                     )
-            rows = jnp.concatenate([box[source, begin:stop, :] for source in sources], axis=0)
+            rows = jnp.concatenate([box[source, a:b, :] for source in sources for a, b in ranges], axis=0)
             for weight, target in ((kw, key_out), (vw, val_out)):
                 made = jnp.dot(rows, weight[...], preferred_element_type=F32).astype(BF16)
                 for n, source in enumerate(sources):
-                    place = pl.ds(pl.multiple_of(source * pos_dev + first, height), height)
+                    place = slice(source * pos_dev + first, source * pos_dev + first + height)
                     for h in range(heads_dev):
                         target[0, h, place, :] = made[
                             n * height:(n + 1) * height, h * key_width:(h + 1) * key_width
@@ -275,14 +273,13 @@
             def _(n=n):
                 part = box.at[0:n]
                 pltpu.make_async_remote_copy(
-                    src_ref=part, dst_ref=part, send_sem=sent.at[index], recv_sem=crecv.at[0, 0],
+                    src_ref=part, dst_ref=part, send_sem=sent.at[index], recv_sem=zrecv.at[0, 0],
                     device_id={"sp": me}, device_id_type=MESH,
                 ).wait_send()
 
     upward = jnp.where(inner[0], (here + 1) * seq_local, 0)
     downward = jnp.where(inner[1], (tp_count - here) * seq_local, 0)
     drain(0, upward + downward, (tp_count + 1) * seq_local if tp_count > 1 else 0)
-    prompts = tp_count * seq_local
     beside = jnp.logical_or(jnp.logical_not(at_end), jnp.abs(me // seq_local - here) <= 1)
     reach = jnp.where(at_end, min(tp_count, 2) * seq_local, prompts)
     drain(1, reach - jnp.where(beside, 1, 0), prompts)
@@ -307,16 +304,15 @@
     total = lax.dot_general(spread, all_keys, (((1,), (1,)), ((), ())), preferred_element_type=F32)
     total = (total + jnp.dot(rotated, ropes[0], preferred_element_type=F32)) * scale
     terms = jnp.exp(total - jnp.max(total, axis=-1, keepdims=True))
-    weights = terms / jnp.sum(terms, axis=-1, keepdims=True)
-    high = weights.astype(BF16).astype(F32)
-    both = jnp.concatenate([high, weights - high], axis=0).astype(BF16)
+    high = terms.astype(BF16).astype(F32)
+    both = jnp.concatenate([high, terms - high], axis=0).astype(BF16)
     all_vals = jnp.concatenate([vals[0, h] for h in range(heads_dev)], axis=1)
     reads = jnp.dot(both, all_vals, preferred_element_type=F32)
     picks = []
     for h in range(heads_dev):
         span = slice(h * key_width, (h + 1) * key_width)
         picks.append(reads[h:h + 1, span] + reads[heads_dev + h:heads_dev + h + 1, span])
-    read[0] = jnp.concatenate(picks, axis=0).astype(BF16)
+    read[0] = (jnp.concatenate(picks, axis=0) / jnp.sum(terms, axis=-1, keepdims=True)).astype(BF16)
     moves.append(pltpu.make_async_copy(read, read_out, sem.at[3]))
     moves[-1].start()
     for move in moves:
@@ -335,7 +331,8 @@
     rope_rows = rope_width * pos_dev // latent_width
     rows = rope_rows + pos_dev
     quarter = pos_dev // 4
-    cuts = (0, quarter, 2 * quarter, 3 * quarter + rope_rows, rows)
+    lead, rope_at = quarter, 2 * quarter
+    cuts = (0, lead, rope_at, rows - quarter // 2, rows)
     groups = ((0, 1), (2,), (3,))
     parts = 4
     prompts = tp_count * seq_local
@@ -347,7 +344,7 @@
     count = len(cuts) - 1
     dma = pltpu.SemaphoreType.DMA
     made = pl.pallas_call(
-        functools.partial(kernel, sp_count, tp_count, heads_dev, cuts, groups, parts),
+        functools.partial(kernel, sp_count, tp_count, heads_dev, lead, rope_at, cuts, groups, parts),
         out_shape=(
             jax.ShapeDtypeStruct((1, heads_dev, length, key_width), BF16),
             jax.ShapeDtypeStruct((1, heads_dev, length, key_width), BF16),
@@ -366,11 +363,11 @@
             pltpu.VMEM((latent_width, heads_dev * key_width), BF16),
             pltpu.VMEM((latent_width, heads_dev * key_width), BF16),
             pltpu.VMEM((2, rope_width // 2, pos_dev), F32),
-            dma((parts, 2)),
-            dma((5,)),
+            dma((parts + 3,)),
             dma((2,)),
             dma((prompts, count)),
             dma((sp_count, len(groups))),
+            pltpu.SemaphoreType.REGULAR((1,)),
         ],
         compiler_params=pltpu.CompilerParams(
             collective_id=0, has_side_effects=True, vmem_limit_bytes=53000000

time: 26.4 us -> 26.1 us (0.989)
  Pallas kernels: 25.6 us -> 25.2 us
    pallas_call x1, Pallas kernels: 24.1 us -> 23.8 us  [local(): pl.pallas_call(functools.partial(kernel, sp_count, tp_count, heads_dev, l...]
where the time goes in v3:
time: 26.1 us; the launch traced here: 25.9 us
  Pallas kernels  25.2 us (97%)
  between operations  0.69 us (3%)
    pallas_call x1, Pallas kernels, local(): pl.pallas_call(functools.partial(kernel, sp_count, tp_count, heads_dev, l...  23.8 us
    pallas_call x1, Pallas kernels, local(): pl.pallas_call(functools.partial(finish, (key_width + rope_width) ** (-0....  1.39 us

profile of v3, /device:TPU:5, one launch (start us, length us, event | category | flops | bytes accessed | tf_op | source)
XLA Modules:
  0.0 25.9 jit_solution(5777144443736150875)
XLA Ops:
  0.6 0.0 copy-start
  0.6 0.0 copy-start.1
  0.7 0.0 copy-start.2
  0.7 23.8 %shard_map.129 = (bf16[1,4,1024,128]{3,2,1,0:T(8,128)(2,1)S(1)}, bf16[1,4,1024,128]{3,2,1,0:T(8,128)(2,1)S(1)}, bf16[1,64,1024]{2,1,0:T(8,128)(2,1)S(1)}) custom-call(bf16[1,256,2048]{2,1,0:T(8,128)(2,1)} %tok.1, bf16[2048,512]{1,0:T(8,128)(2,1)} %kvd.1, bf16[64,2048]{1,0:T(8,128)(2,1)} %bitcast.3, f32[1,512]{1,0:T(1,128)} %bitcast.4, ...), custom_call_target="tpu_custom_call" | custom-call | tf_op jit(solution)/shard_map/pallas_call | solution.py:346
  24.5 0.0 copy-done
  24.5 0.0 copy-done.1
  24.5 0.0 copy-done.2
  24.5 1.4 %shard_map.130 = (bf16[1,4,1024,128]{3,2,1,0:T(8,128)(2,1)}, bf16[1,4,1024,128]{3,2,1,0:T(8,128)(2,1)}, bf16[1,64,1024]{2,1,0:T(8,128)(2,1)}, bf16[1,4,128]{2,1,0:T(4,128)(2,1)}) custom-call(bf16[1,4,1024,128]{3,2,1,0:T(8,128)(2,1)S(1)} %get-tuple-element.11.keys, bf16[1,4,1024,128]{3,2,1,0:T(8,128)(2,1)S(1)} %get-tuple-element.12.vals, ...), custom_call_target="tpu_custom_call" | custom-call | tf_op jit(solution)/shard_map/pallas_call | solution.py:384
Async XLA Ops:
  0.6 23.9 %copy-start = (bf16[1,4,128]{2,1,0:T(4,128)(2,1)S(1)}, bf16[1,4,128]{2,1,0:T(4,128)(2,1)}, u32[]{:S(2)}) copy-start(bf16[1,4,128]{2,1,0:T(4,128)(2,1)} %query.1) | copy-start | bytes 3076
  0.6 23.9 %copy-start.1 = (bf16[1,4,64]{2,1,0:T(4,128)(2,1)S(1)}, bf16[1,4,64]{2,1,0:T(4,128)(2,1)}, u32[]{:S(2)}) copy-start(bf16[1,4,64]{2,1,0:T(4,128)(2,1)} %ask.1) | copy-start | bytes 1540
  0.7 23.9 %copy-start.2 = (f32[2,64]{1,0:T(2,128)S(1)}, f32[2,64]{1,0:T(2,128)}, u32[]{:S(2)}) copy-start(f32[2,64]{1,0:T(2,128)} %constant.5.clone.qtab) | copy-start | bytes 1540

commit v4 on v3

--- a/solution.py
+++ b/solution.py
@@ -98,6 +98,9 @@
             barrier, inc=1, device_id={"sp": lax.rem(me + step, sp_count)}, device_id_type=MESH
         )
 
+    def landing(lane, group):
+        return crecv.at[group + lax.rem(lane, 2) if group == 1 else group + (group > 1)]
+
     def slot(prompt):
         return jnp.where(prompt == me, me, sp_count + prompt)
 
@@ -107,12 +110,12 @@
         if final:
             return pltpu.make_async_remote_copy(
                 src_ref=part, dst_ref=box.at[me, pieces[s]],
-                send_sem=sent.at[0], recv_sem=crecv.at[me, group_of[s]],
+                send_sem=sent.at[0], recv_sem=landing(me, group_of[s]),
                 device_id={"sp": prompt, "tp": tp}, device_id_type=MESH,
             )
         return pltpu.make_async_remote_copy(
             src_ref=part, dst_ref=part,
-            send_sem=sent.at[0], recv_sem=zrecv.at[prompt, s],
+            send_sem=sent.at[0], recv_sem=zrecv.at[prompt - way * seq_local, s],
             device_id={"sp": me, "tp": tp}, device_id_type=MESH,
         )
 
@@ -130,7 +133,7 @@
     def across(prompt, s):
         return pltpu.make_async_remote_copy(
             src_ref=box.at[slot(prompt), pieces[s]], dst_ref=box.at[me, pieces[s]],
-            send_sem=sent.at[1], recv_sem=crecv.at[me, group_of[s]],
+            send_sem=sent.at[1], recv_sem=landing(me, group_of[s]),
             device_id={"sp": prompt}, device_id_type=MESH,
         )
 
@@ -230,12 +233,25 @@
                         def _():
                             across(prompt, s).start()
 
-    def arrived(source, group):
-        part = box.at[source, spans[group]]
-        pltpu.make_async_remote_copy(
-            src_ref=part, dst_ref=part, send_sem=sent.at[1], recv_sem=crecv.at[source, group],
-            device_id={"sp": me}, device_id_type=MESH,
-        ).wait_recv()
+    def arrived(members, group):
+        def wait(blocks):
+            part = box.at[0:blocks, spans[group]]
+            pltpu.make_async_remote_copy(
+                src_ref=part, dst_ref=part, send_sem=sent.at[1], recv_sem=landing(members[0], group),
+                device_id={"sp": me}, device_id_type=MESH,
+            ).wait_recv()
+
+        size = len(members)
+        own = lax.rem(me, 2) == members[0] % 2 if group == 1 else me >= 0
+        every = jnp.logical_or(landed, jnp.logical_not(own))
+
+        @pl.when(every)
+        def _():
+            wait(size)
+        if size > 1:
+            @pl.when(jnp.logical_not(every))
+            def _():
+                wait(size - 1)
 
     landed = jnp.logical_and(at_end, me // seq_local != here)
     for group, members in enumerate(groups):
@@ -246,12 +262,17 @@
         height = sum(b - a for a, b in ranges)
         first = begin if begin <= rope_at else begin - rope_rows
         batch = 4 if group == len(groups) - 1 else 2
+        odds = [lane for lane in lanes if lane % 2]
+        evens = [lane for lane in lanes if lane % 2 == 0]
         for base in range(0, sp_count, batch):
             sources = lanes[base:base + batch]
+            if group != 1 and base == 0:
+                arrived(lanes, group)
+            if group == 1 and odds[0] in sources:
+                arrived(odds, group)
+            if group == 1 and evens[0] in sources:
+                arrived(evens, group)
             for source in sources:
-                @pl.when(jnp.logical_or(me != source, landed))
-                def _(source=source):
-                    arrived(source, group)
                 if with_rope:
                     packed = box[source, rope_at:rope_at + rope_rows, :]
                     rope_out[0, :, source * pos_dev:(source + 1) * pos_dev] = jnp.concatenate(
@@ -365,8 +386,8 @@
             pltpu.VMEM((2, rope_width // 2, pos_dev), F32),
             dma((parts + 3,)),
             dma((2,)),
-            dma((prompts, count)),
-            dma((sp_count, len(groups))),
+            dma((max(prompts - seq_local, 1), count)),
+            dma((len(groups) + 1,)),
             pltpu.SemaphoreType.REGULAR((1,)),
         ],
         compiler_params=pltpu.CompilerParams(

time: 26.1 us -> 26 us (level)
  no operation moved by 1% of the time
where the time goes in v4:
time: 26 us; the launch traced here: 25.8 us
  Pallas kernels  25.1 us (97%)
  between operations  0.69 us (3%)
    pallas_call x1, Pallas kernels, local(): pl.pallas_call(functools.partial(kernel, sp_count, tp_count, heads_dev, l...  23.7 us
    pallas_call x1, Pallas kernels, local(): pl.pallas_call(functools.partial(finish, (key_width + rope_width) ** (-0....  1.39 us

profile of v4, /device:TPU:5, one launch (start us, length us, event | category | flops | bytes accessed | tf_op | source)
XLA Modules:
  0.0 25.8 jit_solution(2077231460887834845)
XLA Ops:
  0.6 0.0 copy-start
  0.6 0.0 copy-start.1
  0.7 0.0 copy-start.2
  0.7 23.7 %shard_map.129 = (bf16[1,4,1024,128]{3,2,1,0:T(8,128)(2,1)S(1)}, bf16[1,4,1024,128]{3,2,1,0:T(8,128)(2,1)S(1)}, bf16[1,64,1024]{2,1,0:T(8,128)(2,1)S(1)}) custom-call(bf16[1,256,2048]{2,1,0:T(8,128)(2,1)} %tok.1, bf16[2048,512]{1,0:T(8,128)(2,1)} %kvd.1, bf16[64,2048]{1,0:T(8,128)(2,1)} %bitcast.3, f32[1,512]{1,0:T(1,128)} %bitcast.4, ...), custom_call_target="tpu_custom_call" | custom-call | tf_op jit(solution)/shard_map/pallas_call | solution.py:367
  24.4 0.0 copy-done
  24.4 0.0 copy-done.1
  24.4 0.0 copy-done.2
  24.4 1.4 %shard_map.130 = (bf16[1,4,1024,128]{3,2,1,0:T(8,128)(2,1)}, bf16[1,4,1024,128]{3,2,1,0:T(8,128)(2,1)}, bf16[1,64,1024]{2,1,0:T(8,128)(2,1)}, bf16[1,4,128]{2,1,0:T(4,128)(2,1)}) custom-call(bf16[1,4,1024,128]{3,2,1,0:T(8,128)(2,1)S(1)} %get-tuple-element.11.keys, bf16[1,4,1024,128]{3,2,1,0:T(8,128)(2,1)S(1)} %get-tuple-element.12.vals, ...), custom_call_target="tpu_custom_call" | custom-call | tf_op jit(solution)/shard_map/pallas_call | solution.py:405
Async XLA Ops:
  0.6 23.8 %copy-start = (bf16[1,4,128]{2,1,0:T(4,128)(2,1)S(1)}, bf16[1,4,128]{2,1,0:T(4,128)(2,1)}, u32[]{:S(2)}) copy-start(bf16[1,4,128]{2,1,0:T(4,128)(2,1)} %query.1) | copy-start | bytes 3076
  0.6 23.8 %copy-start.1 = (bf16[1,4,64]{2,1,0:T(4,128)(2,1)S(1)}, bf16[1,4,64]{2,1,0:T(4,128)(2,1)}, u32[]{:S(2)}) copy-start(bf16[1,4,64]{2,1,0:T(4,128)(2,1)} %ask.1) | copy-start | bytes 1540
  0.7 23.8 %copy-start.2 = (f32[2,64]{1,0:T(2,128)S(1)}, f32[2,64]{1,0:T(2,128)}, u32[]{:S(2)}) copy-start(f32[2,64]{1,0:T(2,128)} %constant.5.clone.qtab) | copy-start | bytes 1540

commit v5 on v4

--- a/solution.py
+++ b/solution.py
@@ -75,8 +75,9 @@
         ], n))
     gains = pltpu.make_async_copy(gain, gain_v, load_sem.at[parts])
     gains.start()
+    following = load([(tok.at[:, lead:rope_at, :], tok_v.at[:, lead:rope_at, :])], parts + 3)
     rest = load([
-        (tok.at[:, lead:pos_dev, :], tok_v.at[:, lead:pos_dev, :]),
+        (tok.at[:, rope_at:pos_dev, :], tok_v.at[:, rope_at:pos_dev, :]),
         (rpt, rpt_v),
         (tab.at[:, :, pl.ds(pl.multiple_of(me * pos_dev, pos_dev), pos_dev)], tab_v),
     ], parts + 1)
@@ -184,9 +185,10 @@
             latent = jnp.dot(tok_v[q, begin:stop, :], kvd_v[...], preferred_element_type=F32)
             box[slot(here * seq_local + q), place:place + stop - begin, :] = normed(latent)
 
-    rest.wait()
+    following.wait()
     finish_rows(lead, rope_at, lead)
     send((1,))
+    rest.wait()
     finish_rows(rope_at, pos_dev, rope_at + rope_rows)
     for q in range(seq_local):
         raw = lax.dot_general(rpt_v[...], tok_v[q], (((1,), (1,)), ((), ())), preferred_element_type=F32)
@@ -253,6 +255,24 @@
             def _():
                 wait(size - 1)
 
+    def drain(index, blocks, most):
+        for n in range(1, most + 1):
+            @pl.when(blocks == n)
+            def _(n=n):
+                part = box.at[0:n]
+                pltpu.make_async_remote_copy(
+                    src_ref=part, dst_ref=part, send_sem=sent.at[index], recv_sem=zrecv.at[0, 0],
+                    device_id={"sp": me}, device_id_type=MESH,
+                ).wait_send()
+
+    def drained():
+        upward = jnp.where(inner[0], (here + 1) * seq_local, 0)
+        downward = jnp.where(inner[1], (tp_count - here) * seq_local, 0)
+        drain(0, upward + downward, (tp_count + 1) * seq_local if tp_count > 1 else 0)
+        beside = jnp.logical_or(jnp.logical_not(at_end), jnp.abs(me // seq_local - here) <= 1)
+        reach = jnp.where(at_end, min(tp_count, 2) * seq_local, prompts)
+        drain(1, reach - jnp.where(beside, 1, 0), prompts)
+
     landed = jnp.logical_and(at_end, me // seq_local != here)
     for group, members in enumerate(groups):
         begin, stop = cuts[members[0]], cuts[members[-1] + 1]
@@ -261,7 +281,10 @@
         ranges = [(a, b) for a, b in ranges if b > a]
         height = sum(b - a for a, b in ranges)
         first = begin if begin <= rope_at else begin - rope_rows
-        batch = 4 if group == len(groups) - 1 else 2
+        batch = 2
+        if group == len(groups) - 1:
+            batch = 4
+            drained()
         odds = [lane for lane in lanes if lane % 2]
         evens = [lane for lane in lanes if lane % 2 == 0]
         for base in range(0, sp_count, batch):
@@ -287,23 +310,6 @@
                         target[0, h, place, :] = made[
                             n * height:(n + 1) * height, h * key_width:(h + 1) * key_width
                         ]
-
-    def drain(index, blocks, most):
-        for n in range(1, most + 1):
-            @pl.when(blocks == n)
-            def _(n=n):
-                part = box.at[0:n]
-                pltpu.make_async_remote_copy(
-                    src_ref=part, dst_ref=part, send_sem=sent.at[index], recv_sem=zrecv.at[0, 0],
-                    device_id={"sp": me}, device_id_type=MESH,
-                ).wait_send()
-
-    upward = jnp.where(inner[0], (here + 1) * seq_local, 0)
-    downward = jnp.where(inner[1], (tp_count - here) * seq_local, 0)
-    drain(0, upward + downward, (tp_count + 1) * seq_local if tp_count > 1 else 0)
-    beside = jnp.logical_or(jnp.logical_not(at_end), jnp.abs(me // seq_local - here) <= 1)
-    reach = jnp.where(at_end, min(tp_count, 2) * seq_local, prompts)
-    drain(1, reach - jnp.where(beside, 1, 0), prompts)
 
 
 def finish(scale, keys, vals, ropes, query, ask, qtab, key_out, val_out, rope_out, read_out, read, sem):
@@ -384,7 +390,7 @@
             pltpu.VMEM((latent_width, heads_dev * key_width), BF16),
             pltpu.VMEM((latent_width, heads_dev * key_width), BF16),
             pltpu.VMEM((2, rope_width // 2, pos_dev), F32),
-            dma((parts + 3,)),
+            dma((parts + 4,)),
             dma((2,)),
             dma((max(prompts - seq_local, 1), count)),
             dma((len(groups) + 1,)),

time: 26 us -> 26 us (level)
  no operation moved by 1% of the time
where the time goes in v5:
time: 26 us; the launch traced here: 25.8 us
  Pallas kernels  25.1 us (97%)
  between operations  0.69 us (3%)
    pallas_call x1, Pallas kernels, local(): pl.pallas_call(functools.partial(kernel, sp_count, tp_count, heads_dev, l...  23.7 us
    pallas_call x1, Pallas kernels, local(): pl.pallas_call(functools.partial(finish, (key_width + rope_width) ** (-0....  1.39 us

profile of v5, /device:TPU:5, one launch (start us, length us, event | category | flops | bytes accessed | tf_op | source)
XLA Modules:
  0.0 25.8 jit_solution(7303182518284457652)
XLA Ops:
  0.6 0.0 copy-start
  0.6 0.0 copy-start.1
  0.7 0.0 copy-start.2
  0.7 23.7 %shard_map.129 = (bf16[1,4,1024,128]{3,2,1,0:T(8,128)(2,1)S(1)}, bf16[1,4,1024,128]{3,2,1,0:T(8,128)(2,1)S(1)}, bf16[1,64,1024]{2,1,0:T(8,128)(2,1)S(1)}) custom-call(bf16[1,256,2048]{2,1,0:T(8,128)(2,1)} %tok.1, bf16[2048,512]{1,0:T(8,128)(2,1)} %kvd.1, bf16[64,2048]{1,0:T(8,128)(2,1)} %bitcast.3, f32[1,512]{1,0:T(1,128)} %bitcast.4, ...), custom_call_target="tpu_custom_call" | custom-call | tf_op jit(solution)/shard_map/pallas_call | solution.py:373
  24.4 0.0 copy-done
  24.4 0.0 copy-done.1
  24.4 0.0 copy-done.2
  24.4 1.4 %shard_map.130 = (bf16[1,4,1024,128]{3,2,1,0:T(8,128)(2,1)}, bf16[1,4,1024,128]{3,2,1,0:T(8,128)(2,1)}, bf16[1,64,1024]{2,1,0:T(8,128)(2,1)}, bf16[1,4,128]{2,1,0:T(4,128)(2,1)}) custom-call(bf16[1,4,1024,128]{3,2,1,0:T(8,128)(2,1)S(1)} %get-tuple-element.11.keys, bf16[1,4,1024,128]{3,2,1,0:T(8,128)(2,1)S(1)} %get-tuple-element.12.vals, ...), custom_call_target="tpu_custom_call" | custom-call | tf_op jit(solution)/shard_map/pallas_call | solution.py:411
Async XLA Ops:
  0.6 23.8 %copy-start = (bf16[1,4,128]{2,1,0:T(4,128)(2,1)S(1)}, bf16[1,4,128]{2,1,0:T(4,128)(2,1)}, u32[]{:S(2)}) copy-start(bf16[1,4,128]{2,1,0:T(4,128)(2,1)} %query.1) | copy-start | bytes 3076
  0.6 23.8 %copy-start.1 = (bf16[1,4,64]{2,1,0:T(4,128)(2,1)S(1)}, bf16[1,4,64]{2,1,0:T(4,128)(2,1)}, u32[]{:S(2)}) copy-start(bf16[1,4,64]{2,1,0:T(4,128)(2,1)} %ask.1) | copy-start | bytes 1540
  0.7 23.8 %copy-start.2 = (f32[2,64]{1,0:T(2,128)S(1)}, f32[2,64]{1,0:T(2,128)}, u32[]{:S(2)}) copy-start(f32[2,64]{1,0:T(2,128)} %constant.5.clone.qtab) | copy-start | bytes 1540
